TPU v7x, 32 devices: a whole 2x2x4 slice. The times are simulated.
32 devices in a mesh: grp: 2 (over y), kv: 4 (over z), tp: 4 (over x, core).
Axes of the slice: x: 2, y: 2, z: 4, core: 2. Of those that a mesh axis runs over, the one named last changes fastest.
Arguments:
- stream_in: bfloat16 [96, 4096], P(('grp', 'tp'), 'kv'), parts along dimension 0, may hold values from -40 to 40
- positions: int32 [96], P(('grp', 'kv')), parts along dimension 0, may hold values from 1024 to 32767
- ret_state: float32 [96, 16, 128, 128], P(('grp', 'kv'), 'tp'), parts along dimension 0, may hold values from -0.6 to 0.6
- first_gain: float32 [4096], P('kv'), may hold values from 0.1 to 1.9
- first_gate: bfloat16 [4096, 11008], P('kv', 'tp'), may hold values from -0.09375 to 0.09375
- first_up: bfloat16 [4096, 11008], P('kv', 'tp'), may hold values from -0.09375 to 0.09375
- first_down: bfloat16 [11008, 4096], P('tp', 'kv'), may hold values from -0.1875 to 0.1875
- mix_gain: float32 [4096], P('kv'), may hold values from 0.1 to 1.9
- w_query: bfloat16 [4096, 2048], P('kv', 'tp'), may hold values from -0.09375 to 0.09375
- w_key: bfloat16 [4096, 2048], P('kv', 'tp'), may hold values from -0.09375 to 0.09375
- w_value: bfloat16 [4096, 2048], P('kv', 'tp'), may hold values from -0.09375 to 0.09375
- w_outgate: bfloat16 [4096, 2048], P('kv', 'tp'), may hold values from -0.09375 to 0.09375
- w_out: bfloat16 [2048, 4096], P('tp', 'kv'), may hold values from -0.21875 to 0.21875
- head_gain: float32 [2048], P('tp'), may hold values from 0.1 to 1.9
- second_gain: float32 [4096], P('kv'), may hold values from 0.1 to 1.9
- second_gate: bfloat16 [4096, 11008], P('kv', 'tp'), may hold values from -0.09375 to 0.09375
- second_up: bfloat16 [4096, 11008], P('kv', 'tp'), may hold values from -0.09375 to 0.09375
- second_down: bfloat16 [11008, 4096], P('tp', 'kv'), may hold values from -0.1875 to 0.1875
Outputs:
- stream_out: bfloat16 [96, 4096], P(('grp', 'tp'), 'kv'), parts along dimension 0
- new_state: float32 [96, 16, 128, 128], P(('grp', 'kv'), 'tp'), parts along dimension 0
There are 2 independent parts, one for each index of `grp`. A program takes and returns all parts, laid end to end along the dimension named above; an argument that names none is the same for every part. Nothing has to cross between parts.
All inputs are finite; a program needn't handle non-finite values.
Results may differ from a plain program's by a relative error of at most 0.03.
Values may be sent and summed in bfloat16 or wider, within the bound.
A program may use at most 128 MiB of HBM per device.

v0:
```python
import jax
import jax.numpy as jnp
from jax import lax
from jax.sharding import PartitionSpec as P

D = 4096


EPS_NORM = 1e-06
EPS_GROUP = 1e-05


def widen_rows(stream_rows):
    return lax.all_gather(stream_rows, "tp", axis=0, tiled=True)


def prepare(stream, norm_gain):
    widened = stream.astype(jnp.float32)
    squares = jnp.sum(widened * widened, axis=1)
    scaled = (widened * norm_gain).astype(jnp.bfloat16)
    return (squares, scaled)


def feed_forward(stream, norm_gain, w_gate, w_up):
    squares, scaled = prepare(stream, norm_gain)
    gate_part = jnp.dot(scaled, w_gate, preferred_element_type=jnp.float32)
    up_part = jnp.dot(scaled, w_up, preferred_element_type=jnp.float32)
    gate_part, up_part, squares = (
        lax.psum(gate_part.astype(jnp.bfloat16), "kv").astype(jnp.float32),
        lax.psum(up_part.astype(jnp.bfloat16), "kv").astype(jnp.float32),
        lax.psum(squares.astype(jnp.bfloat16), "kv").astype(jnp.float32),
    )
    factor = lax.rsqrt(squares / D + EPS_NORM)[:, None]
    return (jax.nn.silu(factor * gate_part) * (factor * up_part)).astype(jnp.bfloat16)


def advance(stream, inputs_back, weight_back, factor_branch):
    row_count = stream.shape[0] // lax.axis_size("tp")
    row_share = lax.psum_scatter(
        jnp.dot(inputs_back, weight_back, preferred_element_type=jnp.float32).astype(jnp.bfloat16),
        "tp",
        scatter_dimension=0,
        tiled=True,
    ).astype(jnp.float32)
    own_rows = lax.dynamic_slice_in_dim(stream, lax.axis_index("tp") * row_count, row_count, 0)
    return (own_rows.astype(jnp.float32) + factor_branch * row_share).astype(jnp.bfloat16)


def rotate(values_in, cosine, sine_part):
    half_dim = values_in.shape[-1] // 2
    lower_half = values_in[..., :half_dim]
    upper_half = values_in[..., half_dim:]
    return jnp.concatenate(
        [
            lower_half * cosine - upper_half * sine_part,
            lower_half * sine_part + upper_half * cosine,
        ],
        axis=-1,
    )


def retention(
    stream, norm_gain, w_query, w_key, w_value, w_outgate, head_gain, state_old, positions
):
    squares, scaled = prepare(stream, norm_gain)
    query_part = jnp.dot(scaled, w_query, preferred_element_type=jnp.float32)
    key_part = jnp.dot(scaled, w_key, preferred_element_type=jnp.float32)
    value_part = jnp.dot(scaled, w_value, preferred_element_type=jnp.float32)
    gate_part = jnp.dot(scaled, w_outgate, preferred_element_type=jnp.float32)
    query_part, key_part, value_part, gate_part, squares = (
        lax.psum_scatter(
            query_part.astype(jnp.bfloat16), "kv", scatter_dimension=0, tiled=True
        ).astype(jnp.float32),
        lax.psum_scatter(
            key_part.astype(jnp.bfloat16), "kv", scatter_dimension=0, tiled=True
        ).astype(jnp.float32),
        lax.psum_scatter(
            value_part.astype(jnp.bfloat16), "kv", scatter_dimension=0, tiled=True
        ).astype(jnp.float32),
        lax.psum_scatter(
            gate_part.astype(jnp.bfloat16), "kv", scatter_dimension=0, tiled=True
        ).astype(jnp.float32),
        lax.psum_scatter(
            squares.astype(jnp.bfloat16), "kv", scatter_dimension=0, tiled=True
        ).astype(jnp.float32),
    )
    factor = lax.rsqrt(squares / D + EPS_NORM)[:, None]
    sequences = state_old.shape[0]
    head_count = state_old.shape[1]
    width_head = state_old.shape[2]
    shape_heads = (sequences, head_count, width_head)
    queries = (factor * query_part).reshape(shape_heads)
    key_vec = (factor * key_part).reshape(shape_heads)
    values_new = (factor * value_part).reshape(shape_heads)
    gate_pre = (factor * gate_part).reshape(shape_heads)
    half_dim = width_head // 2
    inverse = 10000.0 ** (-jnp.arange(half_dim, dtype=jnp.float32) / half_dim)
    angles = positions.astype(jnp.float32)[:, None] * inverse[None, :]
    cosine = jnp.cos(angles)[:, None, :]
    sine_part = jnp.sin(angles)[:, None, :]
    queries = rotate(queries, cosine, sine_part)
    key_vec = rotate(key_vec, cosine, sine_part) * width_head ** (-0.5)
    head_ids = (lax.axis_index("tp") * head_count + jnp.arange(head_count)).astype(jnp.float32)
    decays = jnp.exp(jnp.log1p(-(2.0 ** (-5.0 - head_ids))))
    carried = jnp.einsum("shd,shde->she", queries, state_old, precision=lax.Precision.HIGHEST)
    within = jnp.sum(queries * key_vec, axis=-1, keepdims=True)
    mixture = decays[None, :, None] * carried + within * values_new
    new_state = (
        decays[None, :, None, None] * state_old + key_vec[..., :, None] * values_new[..., None, :]
    )
    average = jnp.mean(mixture, axis=-1, keepdims=True)
    centered = mixture - average
    variance = jnp.mean(centered * centered, axis=-1, keepdims=True)
    normed = centered * lax.rsqrt(variance + EPS_GROUP) * head_gain.reshape(head_count, width_head)
    ret_out = (
        (jax.nn.silu(gate_pre) * normed)
        .astype(jnp.bfloat16)
        .reshape(sequences, head_count * width_head)
    )
    return (lax.all_gather(ret_out, "kv", axis=0, tiled=True), new_state)


def per_device(
    stream_in,
    positions,
    ret_state,
    first_gain,
    first_gate,
    first_up,
    first_down,
    mix_gain,
    w_query,
    w_key,
    w_value,
    w_outgate,
    w_out,
    head_gain,
    second_gain,
    second_gate,
    second_up,
    second_down,
):
    stream = widen_rows(stream_in)
    hidden = feed_forward(stream, first_gain, first_gate, first_up)
    stream = advance(stream, hidden, first_down, 0.5)
    stream = widen_rows(stream)
    ret_out, new_state = retention(
        stream, mix_gain, w_query, w_key, w_value, w_outgate, head_gain, ret_state, positions
    )
    stream = advance(stream, ret_out, w_out, 1.0)
    stream = widen_rows(stream)
    hidden = feed_forward(stream, second_gain, second_gate, second_up)
    stream = advance(stream, hidden, second_down, 0.5)
    return (stream, new_state)


def solution(mesh):
    in_specs = (
        P(("grp", "tp"), "kv"),
        P(("grp", "kv")),
        P(("grp", "kv"), "tp", None, None),
        P("kv"),
        P("kv", "tp"),
        P("kv", "tp"),
        P("tp", "kv"),
        P("kv"),
        P("kv", "tp"),
        P("kv", "tp"),
        P("kv", "tp"),
        P("kv", "tp"),
        P("tp", "kv"),
        P("tp"),
        P("kv"),
        P("kv", "tp"),
        P("kv", "tp"),
        P("tp", "kv"),
    )
    out_specs = (P(("grp", "tp"), "kv"), P(("grp", "kv"), "tp", None, None))
    return jax.shard_map(
        per_device, mesh=mesh, in_specs=in_specs, out_specs=out_specs, check_vma=False
    )
```

profile of v0, /device:TPU:0, one launch (start us, length us, event | category | flops | bytes accessed | tf_op | source)
XLA Modules:
  0.0 234.9 jit_solution(9021519236069175945)
XLA Ops:
  7.2 6.9 %all-gather = bf16[4,12,1024]{2,1,0:T(8,128)(2,1)S(1)} all-gather(bf16[1,12,1024]{2,1,0:T(8,128)(2,1)} %bitcast.43), channel_id=1, replica_groups=mesh['grp'=2,'kv'=4,'tp'=4] {'tp'}, dimensions={0}, use_global_device_ids=true | all-gather | bytes 122880 | tf_op jit(solution)/shard_map/all_gather | solution.py:14
  14.1 5.3 %convolution_convert_fusion.2 = bf16[48,2752]{1,0:T(8,128)(2,1)} fusion(bf16[1024,2752]{0,1:T(8,128)(2,1)} %param.23, bf16[48,1024]{1,0:T(8,128)(2,1)S(1)} %reshape.132, f32[1024]{0:T(1024)} %param.21), kind=kOutput, calls=%fused_computation.3 | convolution fusion | flops 270812160 | bytes 6002688 | tf_op jit(solution)/shard_map/dot_general | solution.py:27
  19.4 2.5 %convolution_convert_fusion.3 = bf16[48,2752]{1,0:T(8,128)(2,1)} fusion(bf16[1024,2752]{0,1:T(8,128)(2,1)S(1)} %copy-done.1, bf16[48,1024]{1,0:T(8,128)(2,1)S(1)} %reshape.132, f32[1024]{0:T(1024)S(1)} %copy-done.5), kind=kOutput, calls=%fused_computation.4 | convolution fusion | flops 270812160 | bytes 6002688 | tf_op jit(solution)/shard_map/dot_general | solution.py:26
  22.0 0.1 fusion.14
  22.2 12.6 %psum.42 = bf16[48]{0:T(256)(128)(2,1)S(1)} all-reduce(bf16[48]{0:T(256)(128)(2,1)S(1)} %fusion.14), channel_id=1, replica_groups=mesh['grp'=2,'kv'=4,'tp'=4] {'kv'}, use_global_device_ids=true, to_apply=%region_1.0 | all-reduce | flops 48 | bytes 192 | tf_op jit(solution)/shard_map/psum | solution.py:31
  34.9 27.7 %all-reduce.23.cloned.1.call-done = (bf16[48,2752]{1,0:T(8,128)(2,1)}, bf16[48,2752]{1,0:T(8,128)(2,1)}) async-done(((bf16[48,2752]{1,0:T(8,128)(2,1)}, bf16[48,2752]{1,0:T(8,128)(2,1)}), (bf16[48,2752]{1,0:T(8,128)(2,1)}, bf16[48,2752]{1,0:T(8,128)(2,1)})) %all-reduce.23.cloned.1.call-update) | async-done | bytes 528400 | tf_op jit(solution)/shard_map/psum | solution.py:30
  62.6 3.9 %convolution_convert_fusion.6 = bf16[48,1024]{1,0:T(8,128)(2,1)S(1)} fusion(bf16[2752,1024]{1,0:T(8,128)(2,1)} %param.24, bf16[48,2752]{1,0:T(8,128)(2,1)} %get-tuple-element.4, bf16[48,2752]{1,0:T(8,128)(2,1)} %get-tuple-element.5, f32[48]{0:T(128)S(1)} %add_rsqrt_fusion.2), kind=kOutput, calls=%fused_computation.8 | convolution fusion | flops 271902720 | bytes 6262976 | tf_op jit(solution)/shard_map/dot_general | solution.py:40
  66.6 8.2 %fusion = bf16[16,1024]{1,0:T(8,128)(2,1)S(1)} fusion(bf16[48,1024]{1,0:T(8,128)(2,1)S(1)} %convolution_convert_fusion.6), kind=kCustom, calls=%all-reduce-scatter | all-reduce-scatter fusion | flops 65537 | bytes 131584
  74.7 1.3 collective-permute-start
  76.1 0.6 dynamic-slice.18
  77.3 0.6 fusion.39
  79.2 0.2 concatenate.12
  79.5 5.7 %all-gather.1 = bf16[4,12,1024]{2,1,0:T(8,128)(2,1)S(1)} all-gather(bf16[1,12,1024]{2,1,0:T(8,128)(2,1)S(1)} %fusion.28), channel_id=1, replica_groups=mesh['grp'=2,'kv'=4,'tp'=4] {'tp'}, dimensions={0}, use_global_device_ids=true | all-gather | bytes 122880 | tf_op jit(solution)/shard_map/all_gather | solution.py:14
  85.3 10.7 %all-reduce.1 = bf16[48]{0:T(256)(128)(2,1)S(1)} all-reduce(bf16[48]{0:T(256)(128)(2,1)S(1)} %fusion.16), channel_id=3, replica_groups=mesh['grp'=2,'kv'=4,'tp'=4] {'kv'}, use_global_device_ids=true, to_apply=%region_6.7.clone | all-reduce | flops 48 | bytes 192
  96.0 0.3 convolution_convert_fusion.9
  96.3 0.3 convolution_convert_fusion.8
  96.6 1.5 convolution_convert_fusion.7
  98.1 1.5 convolution_convert_fusion.10
  99.6 11.4 %fusion.38 = (bf16[16,512]{1,0:T(8,128)(2,1)S(1)}, bf16[16,512]{1,0:T(8,128)(2,1)S(1)}, bf16[16,512]{1,0:T(8,128)(2,1)S(1)}, bf16[16,512]{1,0:T(8,128)(2,1)S(1)}) fusion(bf16[48,512]{1,0:T(8,128)(2,1)S(1)} %convolution_convert_fusion.10, bf16[48,512]{1,0:T(8,128)(2,1)S(1)} %convolution_convert_fusion.7, bf16[48,512]{1,0:T(8,128)(2,1)S(1)} %convolution_convert_fusion.9, ...), kind=kCustom, calls=%all-reduce-scatter.7 | all-reduce-scatter fusion | flops 131073 | bytes 262656
  111.1 3.5 %collective-permute-start.3 = (bf16[12,512]{1,0:T(8,128)(2,1)S(1)}, bf16[12,512]{1,0:T(8,128)(2,1)S(1)}, u32[]{:S(2)}, u32[]{:S(2)}) collective-permute-start(bf16[12,512]{1,0:T(8,128)(2,1)S(1)} %slice.23), channel_id=1, source_target_pairs={{0,4},{4,8},{8,12},{1,5},{5,9},{9,13},{2,6},{6,10},{10,14},{3,7},{... | collective-permute-start | bytes 36872
  114.6 1.9 collective-permute-start.2
  116.5 3.8 %collective-permute-start.4 = (bf16[12,512]{1,0:T(8,128)(2,1)S(1)}, bf16[12,512]{1,0:T(8,128)(2,1)S(1)}, u32[]{:S(2)}, u32[]{:S(2)}) collective-permute-start(bf16[12,512]{1,0:T(8,128)(2,1)S(1)} %slice.24), channel_id=1, source_target_pairs={{0,4},{4,8},{8,12},{1,5},{5,9},{9,13},{2,6},{6,10},{10,14},{3,7},{... | collective-permute-start | bytes 36872
  120.3 1.9 collective-permute-start.1
  122.4 0.1 concatenate.15
  122.5 0.2 concatenate.14
  122.7 0.2 concatenate.16
  122.9 0.8 collective-permute-done.1
  124.2 4.6 %fusion.41 = f32[12,4,1,128]{3,2,1,0:T(1,128)S(1)} fusion(f32[12,4,128,1]{2,3,1,0:T(1,128)S(1)} %bitcast.42, f32[12,4,128,128]{3,2,1,0:T(8,128)} %param.20), kind=kOutput, calls=%fused_computation.70 | convolution fusion | flops 9437184 | bytes 3194880 | tf_op jit(solution)/shard_map/shd,shde->she/dot_general | solution.py:105
  128.8 0.2 fusion.40
  129.0 0.2 multiply_reduce_fusion
  129.3 13.1 %all-gather.2 = bf16[4,12,512]{2,1,0:T(8,128)(2,1)S(1)} all-gather(bf16[1,12,512]{2,1,0:T(8,128)(2,1)S(1)} %reshape.135), channel_id=1, replica_groups=mesh['grp'=2,'kv'=4,'tp'=4] {'kv'}, dimensions={0}, use_global_device_ids=true | all-gather | bytes 61440 | tf_op jit(solution)/shard_map/all_gather | solution.py:120
  142.5 0.3 convolution_convert_fusion.5
  142.8 7.9 %fusion.5 = bf16[16,1024]{1,0:T(8,128)(2,1)S(1)} fusion(bf16[48,1024]{1,0:T(8,128)(2,1)S(1)} %convolution_convert_fusion.5), kind=kCustom, calls=%all-reduce-scatter.5 | all-reduce-scatter fusion | flops 65537 | bytes 131584
  150.7 1.3 collective-permute-start.5
  152.0 0.8 collective-permute-done.5
  152.9 0.1 concatenate.17
  153.0 7.6 %all-gather.3 = bf16[4,12,1024]{2,1,0:T(8,128)(2,1)S(1)} all-gather(bf16[1,12,1024]{2,1,0:T(8,128)(2,1)S(1)} %fusion.29), channel_id=1, replica_groups=mesh['grp'=2,'kv'=4,'tp'=4] {'tp'}, dimensions={0}, use_global_device_ids=true | all-gather | bytes 122880 | tf_op jit(solution)/shard_map/all_gather | solution.py:14
  160.7 5.1 %convolution_convert_fusion = bf16[48,2752]{1,0:T(8,128)(2,1)} fusion(bf16[1024,2752]{0,1:T(8,128)(2,1)} %param.34, bf16[48,1024]{1,0:T(8,128)(2,1)S(1)} %reshape.138, f32[1024]{0:T(1024)S(1)} %copy-done.6), kind=kOutput, calls=%fused_computation.1 | convolution fusion | flops 270812160 | bytes 6002688 | tf_op jit(solution)/shard_map/dot_general | solution.py:27
  165.8 5.1 %convolution_convert_fusion.1 = bf16[48,2752]{1,0:T(8,128)(2,1)} fusion(bf16[1024,2752]{0,1:T(8,128)(2,1)} %param.33, bf16[48,1024]{1,0:T(8,128)(2,1)S(1)} %reshape.138, f32[1024]{0:T(1024)S(1)} %copy-done.6), kind=kOutput, calls=%fused_computation.2 | convolution fusion | flops 270812160 | bytes 6002688 | tf_op jit(solution)/shard_map/dot_general | solution.py:26
  170.9 0.1 fusion.18
  171.1 10.7 %psum.45 = bf16[48]{0:T(256)(128)(2,1)S(1)} all-reduce(bf16[48]{0:T(256)(128)(2,1)S(1)} %fusion.18), channel_id=1, replica_groups=mesh['grp'=2,'kv'=4,'tp'=4] {'kv'}, use_global_device_ids=true, to_apply=%region_16.17 | all-reduce | flops 48 | bytes 192 | tf_op jit(solution)/shard_map/psum | solution.py:31
  181.7 28.4 %all-reduce.21.cloned.1.call-done = (bf16[48,2752]{1,0:T(8,128)(2,1)}, bf16[48,2752]{1,0:T(8,128)(2,1)}) async-done(((bf16[48,2752]{1,0:T(8,128)(2,1)}, bf16[48,2752]{1,0:T(8,128)(2,1)}), (bf16[48,2752]{1,0:T(8,128)(2,1)}, bf16[48,2752]{1,0:T(8,128)(2,1)})) %all-reduce.21.cloned.1.call-update) | async-done | bytes 528400 | tf_op jit(solution)/shard_map/psum | solution.py:30
  210.2 3.9 %convolution_convert_fusion.4 = bf16[48,1024]{1,0:T(8,128)(2,1)S(1)} fusion(bf16[2752,1024]{1,0:T(8,128)(2,1)} %param.35, bf16[48,2752]{1,0:T(8,128)(2,1)} %get-tuple-element.2, bf16[48,2752]{1,0:T(8,128)(2,1)} %get-tuple-element.3, f32[48]{0:T(128)S(1)} %add_rsqrt_fusion.1), kind=kOutput, calls=%fused_computation.6 | convolution fusion | flops 271902720 | bytes 6262976 | tf_op jit(solution)/shard_map/dot_general | solution.py:40
  214.1 8.2 %fusion.6 = bf16[16,1024]{1,0:T(8,128)(2,1)S(1)} fusion(bf16[48,1024]{1,0:T(8,128)(2,1)S(1)} %convolution_convert_fusion.4), kind=kCustom, calls=%all-reduce-scatter.6 | all-reduce-scatter fusion | flops 65537 | bytes 131584
  222.3 1.3 collective-permute-start.6
  223.6 3.6 %multiply_add_fusion = f32[12,4,128,128]{3,2,1,0:T(8,128)} fusion(f32[12,4,128,128]{3,2,1,0:T(8,128)} %param.20, f32[12,4,128]{2,1,0:T(4,128)S(1)} %reshape.129, f32[12,4,128]{2,1,0:T(4,128)S(1)} %get-tuple-element.31, f32[4]{0:T(128)S(1)} %log-plus-one_exponential_fusion), kind=kLoop, calls=%fused_computation.5 | loop fusion | flops 2359296 | bytes 6340624 | tf_op jit(solution)/shard_map/add | solution.py:109
  227.2 0.2 concatenate.18
  227.4 0.7 add_convert_fusion
  (64 shorter events, 1.3 us)
Async XLA Ops:
  7.2 135.3 %copy-start = (bf16[512,1024]{1,0:T(8,128)(2,1)S(1)}, bf16[512,1024]{1,0:T(8,128)(2,1)}, u32[]{:S(2)}) copy-start(bf16[512,1024]{1,0:T(8,128)(2,1)} %param.30) | copy-start | bytes 3145732
  7.2 12.2 %copy-start.5 = (f32[1024]{0:T(1024)S(1)}, f32[1024]{0:T(1024)}, u32[]{:S(2)}) copy-start(f32[1024]{0:T(1024)} %param.21) | copy-start | bytes 12292
  7.2 55.4 %all-reduce.23.cloned.1.call-start = ((), (), s32[]{:S(2)}) async-start(), calls=%async_computation.1 | async-start | bytes 1081344 | tf_op jit(solution)/shard_map/psum | solution.py:30
  14.1 5.3 %copy-start.1 = (bf16[1024,2752]{0,1:T(8,128)(2,1)S(1)}, bf16[1024,2752]{0,1:T(8,128)(2,1)}, u32[]{:S(2)}) copy-start(bf16[1024,2752]{0,1:T(8,128)(2,1)} %param.22) | copy-start | bytes 16908292
  14.1 8.0 %copy-start.10 = (s32[12]{0:T(128)S(1)}, s32[12]{0:T(128)}, u32[]{:S(2)}) copy-start(s32[12]{0:T(128)} %param.19) | copy-start | bytes 148
  19.4 56.7 %copy-start.9 = (u32[32]{0:T(128)S(1)}, u32[32]{0:T(128)}, u32[]{:S(2)}) copy-start(u32[32]{0:T(128)} %constant.53) | copy-start | bytes 388
  19.4 57.9 %copy-start.8 = (u32[32]{0:T(128)S(1)}, u32[32]{0:T(128)}, u32[]{:S(2)}) copy-start(u32[32]{0:T(128)} %constant.57) | copy-start | bytes 388
  21.9 74.0 %copy-start.2 = (bf16[1024,512]{1,0:T(8,128)(2,1)S(1)}, bf16[1024,512]{1,0:T(8,128)(2,1)}, u32[]{:S(2)}) copy-start(bf16[1024,512]{1,0:T(8,128)(2,1)} %param.26) | copy-start | bytes 3145732
  21.9 74.0 %copy-start.4 = (f32[1024]{0:T(1024)S(1)}, f32[1024]{0:T(1024)}, u32[]{:S(2)}) copy-start(f32[1024]{0:T(1024)} %param.25) | copy-start | bytes 12292
  21.9 74.3 %copy-start.3 = (bf16[1024,512]{1,0:T(8,128)(2,1)S(1)}, bf16[1024,512]{1,0:T(8,128)(2,1)}, u32[]{:S(2)}) copy-start(bf16[1024,512]{1,0:T(8,128)(2,1)} %param.27) | copy-start | bytes 3145732
  22.0 188.2 %all-reduce.21.cloned.1.call-start = ((), (), s32[]{:S(2)}) async-start(), calls=%async_computation | async-start | bytes 1081344 | tf_op jit(solution)/shard_map/psum | solution.py:30
  66.5 62.6 %copy-start.7 = (f32[512]{0:T(512)S(1)}, f32[512]{0:T(512)}, u32[]{:S(2)}) copy-start(f32[512]{0:T(512)} %param.31) | copy-start | bytes 6148
  74.7 4.5 %collective-permute-start = (bf16[12,1024]{1,0:T(8,128)(2,1)S(1)}, bf16[12,1024]{1,0:T(8,128)(2,1)S(1)}, u32[]{:S(2)}, u32[]{:S(2)}) collective-permute-start(bf16[12,1024]{1,0:T(8,128)(2,1)S(1)} %slice.20), channel_id=1, source_target_pairs={{0,1},{1,2},{2,3},{4,5},{5,6},{6,7},{8,9},{9,10},{10,11},{12,13},{... | collective-permute-start | bytes 73736
  96.3 64.4 %copy-start.6 = (f32[1024]{0:T(1024)S(1)}, f32[1024]{0:T(1024)}, u32[]{:S(2)}) copy-start(f32[1024]{0:T(1024)} %param.32) | copy-start | bytes 12292
  111.1 11.3 %collective-permute-start.3 = (bf16[12,512]{1,0:T(8,128)(2,1)S(1)}, bf16[12,512]{1,0:T(8,128)(2,1)S(1)}, u32[]{:S(2)}, u32[]{:S(2)}) collective-permute-start(bf16[12,512]{1,0:T(8,128)(2,1)S(1)} %slice.23), channel_id=1, source_target_pairs={{0,4},{4,8},{8,12},{1,5},{5,9},{9,13},{2,6},{6,10},{10,14},{3,7},{... | collective-permute-start | bytes 36872
  114.6 7.9 %collective-permute-start.2 = (bf16[12,512]{1,0:T(8,128)(2,1)S(1)}, bf16[12,512]{1,0:T(8,128)(2,1)S(1)}, u32[]{:S(2)}, u32[]{:S(2)}) collective-permute-start(bf16[12,512]{1,0:T(8,128)(2,1)S(1)} %slice.22), channel_id=1, source_target_pairs={{0,4},{4,8},{8,12},{1,5},{5,9},{9,13},{2,6},{6,10},{10,14},{3,7},{... | collective-permute-start | bytes 36872
  116.5 6.2 %collective-permute-start.4 = (bf16[12,512]{1,0:T(8,128)(2,1)S(1)}, bf16[12,512]{1,0:T(8,128)(2,1)S(1)}, u32[]{:S(2)}, u32[]{:S(2)}) collective-permute-start(bf16[12,512]{1,0:T(8,128)(2,1)S(1)} %slice.24), channel_id=1, source_target_pairs={{0,4},{4,8},{8,12},{1,5},{5,9},{9,13},{2,6},{6,10},{10,14},{3,7},{... | collective-permute-start | bytes 36872
  120.3 3.4 %collective-permute-start.1 = (bf16[12,512]{1,0:T(8,128)(2,1)S(1)}, bf16[12,512]{1,0:T(8,128)(2,1)S(1)}, u32[]{:S(2)}, u32[]{:S(2)}) collective-permute-start(bf16[12,512]{1,0:T(8,128)(2,1)S(1)} %slice.21), channel_id=1, source_target_pairs={{0,4},{4,8},{8,12},{1,5},{5,9},{9,13},{2,6},{6,10},{10,14},{3,7},{... | collective-permute-start | bytes 36872
  150.7 2.1 collective-permute-start.5
  222.3 4.9 %collective-permute-start.6 = (bf16[12,1024]{1,0:T(8,128)(2,1)S(1)}, bf16[12,1024]{1,0:T(8,128)(2,1)S(1)}, u32[]{:S(2)}, u32[]{:S(2)}) collective-permute-start(bf16[12,1024]{1,0:T(8,128)(2,1)S(1)} %slice.26), channel_id=1, source_target_pairs={{0,1},{1,2},{2,3},{4,5},{5,6},{6,7},{8,9},{9,10},{10,11},{12,13},{... | collective-permute-start | bytes 73736
Sparse Core Ops, SparseCore 0:
  22.1 40.4 all-reduce.22
  171.1 39.0 all-reduce.20
where the time goes:
time: 237 us; the launch traced here: 235 us
  blocking collectives  103 us (43%)
  waiting for transfers between devices  57.8 us (24%)
  matrix products  34.3 us (14%)
  between operations  16.5 us (7%)
  starting transfers between devices  15.1 us (6%)
  other arithmetic  5.63 us (2%)
  local copies, waits for them, and re-layouts  2.53 us (1%)
    psum x2, waiting for transfers between devices, feed_forward(): lax.psum(up_part.astype(jnp.bfloat16), 'kv').astype(jnp.float32)  56.1 us
    unnamed x5, blocking collectives  46.3 us
    psum x2, blocking collectives, feed_forward(): lax.psum(squares.astype(jnp.bfloat16), 'kv').astype(jnp.float32)  23.3 us
    all_gather x3, blocking collectives, widen_rows(): return lax.all_gather(stream_rows, 'tp', axis=0, tiled=True)  20.1 us
    unnamed x7, starting transfers between devices  15 us
    all_gather x1, blocking collectives, retention(): return (lax.all_gather(ret_out, 'kv', axis=0, tiled=True), new_state)  13.1 us
    dot_general x2, matrix products, feed_forward(): up_part = jnp.dot(scaled, w_up, preferred_element_type=jnp.float32)  10.4 us
    dot_general x3, matrix products, advance(): jnp.dot(inputs_back, weight_back, preferred_element_type=jnp.float32)  8.18 us
  transfers between devices with their start and end apart: 9, of which 4 were waited for; matrix products, arithmetic and copies ran while one was open for 2% of the time, Pallas kernels for 0%

commit v1 on v0

v1 whole, which is shorter than its diff:
```python
import functools

import jax
import jax.numpy as jnp
import numpy as np
from jax import lax
from jax.experimental import pallas as pl
from jax.experimental.pallas import tpu as pltpu
from jax.sharding import PartitionSpec as P

MESH = pl.DeviceIdType.MESH
EPS_NORM = 1e-06
EPS_GROUP = 1e-05
PIECE = 256
F32 = jnp.float32
BF16 = jnp.bfloat16


def silu(v):
    return v / (1.0 + jnp.exp(-v))


def layer_kernel(
    kv, tp, share,
    stream_ref, cos_ref, sin_ref, gain1_ref, gain_mix_ref, gain2_ref, head_gain_ref,
    gate1_hbm, up1_hbm, down1_hbm, wq_hbm, wk_hbm, wv_hbm, wg_hbm, wo_hbm,
    gate2_hbm, up2_hbm, down2_hbm, state_hbm,
    out_ref, key_out_ref, value_out_ref,
    gate1, up1, down1, wq, wk, wv, wg, wo, gate2, up2, down2, state,
    stream_slots, part_send, part_recv, wide, lhs, acc, sq_slots, inverse,
    ff_send, ff_recv, hidden, proj, proj_send, proj_recv, row_sq, row_sq_send, row_sq_recv,
    padded, carried, ret_slots, mixed,
    load_sem, tp_send_sem, tp_recv_sem, sq_send_sem, sq_recv_sem,
    ff_send_sem, ff_recv_sem, hid_send_sem, hid_recv_sem,
    proj_send_sem, proj_recv_sem, row_send_sem, row_recv_sem, ret_send_sem, ret_recv_sem,
):
    me_k = lax.axis_index("kv")
    me_t = lax.axis_index("tp")
    rows, width = wide.shape
    model = width * kv
    units = gate1.shape[1]
    pieces = -(-units // PIECE)
    ragged = units - (pieces - 1) * PIECE
    rows_t = rows // tp
    rows_k = rows // kv
    half = max(1, kv // 2)
    heads = state.shape[1]
    hd = state.shape[2]
    qw = heads * hd

    loads = []
    order = [
        (gate1_hbm, gate1), (up1_hbm, up1), (down1_hbm, down1), (wq_hbm, wq), (wk_hbm, wk),
        (wv_hbm, wv), (wg_hbm, wg), (state_hbm, state), (wo_hbm, wo),
        (gate2_hbm, gate2), (up2_hbm, up2), (down2_hbm, down2),
    ]
    for n, (src, dst) in enumerate(order):
        copy = pltpu.make_async_copy(src, dst, load_sem.at[n])
        copy.start()
        loads.append(copy)

    barrier = pltpu.get_barrier_semaphore()
    for j in range(1, kv):
        pl.semaphore_signal(barrier, 1, device_id={"kv": lax.rem(me_k + j, kv)}, device_id_type=MESH)
    for j in range(1, tp):
        pl.semaphore_signal(barrier, 1, device_id={"tp": lax.rem(me_t + j, tp)}, device_id_type=MESH)
    pl.semaphore_wait(barrier, kv + tp - 2)

    pending = []

    def exchange(axis, me, n, src_of, dst, send_sem, recv_sem):
        for j in range(1, n):
            dest = lax.rem(me + j, n)
            copy = pltpu.make_async_remote_copy(
                src_ref=src_of(dest), dst_ref=dst.at[me],
                send_sem=send_sem.at[dest], recv_sem=recv_sem.at[me],
                device_id={axis: dest}, device_id_type=MESH,
            )
            copy.start()
            pending.append(copy)

        def arrive():
            for j in range(1, n):
                source = lax.rem(me + j, n)
                pltpu.make_async_remote_copy(
                    src_ref=dst.at[source], dst_ref=dst.at[source],
                    send_sem=send_sem.at[source], recv_sem=recv_sem.at[source],
                    device_id={axis: source}, device_id_type=MESH,
                ).wait_recv()

        return arrive

    def gather_stream(phase):
        slots = stream_slots.at[phase]
        return exchange(
            "tp", me_t, tp, lambda dest: slots.at[me_t], slots,
            tp_send_sem.at[phase], tp_recv_sem.at[phase],
        )

    def widen(phase, arrive, gain_ref):
        arrive()
        for t in range(tp):
            wide[t * rows_t : (t + 1) * rows_t, :] = stream_slots[phase, t].astype(F32)
        stream = wide[...]
        lhs[...] = (stream * gain_ref[...]).astype(BF16)
        return jnp.sum(stream * stream, axis=1, keepdims=True)

    def order_of(k):
        side = lax.rem(me_k // half + 1 + k // half, 2) if kv > 1 else 0
        return side * half + lax.rem(lax.rem(me_k, half) + 1 + lax.rem(k, half), half)

    def advance(phase, factor, last):
        for t in range(tp):
            part_send[phase, t] = acc[t * rows_t : (t + 1) * rows_t, :].astype(BF16)
        slots = part_recv.at[phase]
        arrive = exchange(
            "tp", me_t, tp, lambda dest: part_send.at[phase, dest], slots,
            tp_send_sem.at[3 + phase], tp_recv_sem.at[3 + phase],
        )
        total = part_send[phase, me_t].astype(F32)
        arrive()
        for j in range(1, tp):
            total = total + part_recv[phase, lax.rem(me_t + j, tp)].astype(F32)
        fresh = (stream_slots[phase, me_t].astype(F32) + factor * total).astype(BF16)
        if last:
            out_ref[...] = fresh
            return None
        stream_slots[phase + 1, me_t] = fresh
        return gather_stream(phase + 1)

    def feed_forward(block, phase, arrive, gain_ref, w_gate, w_up, w_down, waits):
        squares = widen(phase, arrive, gain_ref)
        sq_slots[block, me_k] = jnp.broadcast_to(squares, (rows, 128))
        sq = sq_slots.at[block]
        sq_arrive = exchange(
            "kv", me_k, kv, lambda dest: sq.at[me_k], sq, sq_send_sem.at[block], sq_recv_sem.at[block]
        )
        waits[0].wait()
        waits[1].wait()

        def piece_copy(dest, p):
            return pltpu.make_async_remote_copy(
                src_ref=ff_send.at[block, dest, p], dst_ref=ff_recv.at[block, me_k, p],
                send_sem=ff_send_sem.at[block, dest, p], recv_sem=ff_recv_sem.at[block, me_k, p],
                device_id={"kv": dest}, device_id_type=MESH,
            )

        def on_piece(i, _):
            dest = order_of(i // share)
            p = lax.rem(i, share)
            g = dest * share + p

            def multiply(columns, n):
                left = lhs[...]
                for which, w in enumerate((w_gate, w_up)):
                    ff_send[block, dest, p, which, :, 0:n] = jnp.dot(
                        left, w[:, columns], preferred_element_type=F32
                    ).astype(BF16)

            @pl.when(g < pieces - 1)
            def _():
                multiply(pl.ds(pl.multiple_of(g * PIECE, PIECE), PIECE), PIECE)

            @pl.when(g == pieces - 1)
            def _():
                if ragged < PIECE:
                    for which in range(2):
                        ff_send[block, dest, p, which] = jnp.zeros((rows, PIECE), BF16)
                multiply(slice((pieces - 1) * PIECE, units), ragged)

            @pl.when((g < pieces) & (dest != me_k))
            def _():
                piece_copy(dest, p).start()

            return 0

        lax.fori_loop(0, kv * share, on_piece, 0)
        sq_arrive()
        total = sq_slots[block, 0]
        for k in range(1, kv):
            total = total + sq_slots[block, k]
        inverse[...] = lax.rsqrt(total / model + EPS_NORM)

        def hidden_copy(dest, p):
            slot = hidden.at[block, me_k * share + p]
            return pltpu.make_async_remote_copy(
                src_ref=slot, dst_ref=slot,
                send_sem=hid_send_sem.at[block, dest, p], recv_sem=hid_recv_sem.at[block, me_k, p],
                device_id={"kv": dest}, device_id_type=MESH,
            )

        def on_shard(p, _):
            @pl.when(me_k * share + p < pieces)
            def _():
                for j in range(1, kv):
                    source = lax.rem(me_k + j, kv)
                    slot = ff_recv.at[block, source, p]
                    pltpu.make_async_remote_copy(
                        src_ref=slot, dst_ref=slot,
                        send_sem=ff_send_sem.at[block, source, p],
                        recv_sem=ff_recv_sem.at[block, source, p],
                        device_id={"kv": source}, device_id_type=MESH,
                    ).wait_recv()
                sums = []
                for which in range(2):
                    total = ff_send[block, me_k, p, which].astype(F32)
                    for j in range(1, kv):
                        total = total + ff_recv[block, lax.rem(me_k + j, kv), p, which].astype(F32)
                    sums.append(total * inverse[:, 0:1])
                hidden[block, me_k * share + p] = (silu(sums[0]) * sums[1]).astype(BF16)
                for j in range(1, kv):
                    hidden_copy(order_of(j - 1), p).start()

            return 0

        lax.fori_loop(0, share, on_shard, 0)
        acc[...] = jnp.zeros_like(acc)
        waits[2].wait()

        def on_hidden(i, _):
            source = order_of(kv - 1 - i // share)
            p = lax.rem(i, share)
            g = source * share + p

            @pl.when((g < pieces) & (source != me_k))
            def _():
                slot = hidden.at[block, g]
                pltpu.make_async_remote_copy(
                    src_ref=slot, dst_ref=slot,
                    send_sem=hid_send_sem.at[block, source, p],
                    recv_sem=hid_recv_sem.at[block, source, p],
                    device_id={"kv": source}, device_id_type=MESH,
                ).wait_recv()

            @pl.when(g < pieces - 1)
            def _():
                depth = pl.ds(pl.multiple_of(g * PIECE, PIECE), PIECE)
                acc[...] += jnp.dot(hidden[block, g], w_down[depth, :], preferred_element_type=F32)

            @pl.when(g == pieces - 1)
            def _():
                acc[...] += jnp.dot(
                    hidden[block, pieces - 1, :, 0:ragged],
                    w_down[(pieces - 1) * PIECE : units, :],
                    preferred_element_type=F32,
                )

            return 0

        lax.fori_loop(0, kv * share, on_hidden, 0)

        def finish():
            def on_sent(i, _):
                dest = order_of(i // share)
                p = lax.rem(i, share)

                @pl.when((dest * share + p < pieces) & (dest != me_k))
                def _():
                    piece_copy(dest, p).wait_send()

                @pl.when((me_k * share + p < pieces) & (dest != me_k))
                def _():
                    hidden_copy(dest, p).wait_send()

                return 0

            lax.fori_loop(0, kv * share, on_sent, 0)

        return finish

    stream_slots[0, me_t] = stream_ref[...]
    arrive = gather_stream(0)
    finish1 = feed_forward(0, 0, arrive, gain1_ref, gate1, up1, down1, loads[0:3])
    arrive = advance(0, 0.5, False)

    squares = widen(1, arrive, gain_mix_ref)
    row_sq[...] = jnp.broadcast_to(squares, (rows, 128))
    for k in range(kv):
        row_sq_send[k] = row_sq[k * rows_k : (k + 1) * rows_k, :]
    row_arrive = exchange(
        "kv", me_k, kv, lambda dest: row_sq_send.at[dest], row_sq_recv, row_send_sem, row_recv_sem
    )
    arrivals = []
    for n, w in enumerate((wq, wk, wv, wg)):
        loads[3 + n].wait()
        proj[...] = jnp.dot(lhs[...], w[...], preferred_element_type=F32)
        for k in range(kv):
            proj_send[n, k] = proj[k * rows_k : (k + 1) * rows_k, :].astype(BF16)
        arrivals.append(
            exchange(
                "kv", me_k, kv, lambda dest, n=n: proj_send.at[n, dest], proj_recv.at[n],
                proj_send_sem.at[n], proj_recv_sem.at[n],
            )
        )
    loads[7].wait()
    row_arrive()
    total = row_sq_send[me_k]
    for j in range(1, kv):
        total = total + row_sq_recv[lax.rem(me_k + j, kv)]
    factor = lax.rsqrt(total / model + EPS_NORM)[:, 0:1]

    def projected(n):
        arrivals[n]()
        value = proj_send[n, me_k].astype(F32)
        for j in range(1, kv):
            value = value + proj_recv[n, lax.rem(me_k + j, kv)].astype(F32)
        return value * factor

    cosine, sine = cos_ref[...], sin_ref[...]

    def rotated(value, scale):
        parts = []
        for h in range(heads):
            x = value[:, h * hd : (h + 1) * hd]
            parts.append((x * cosine + pltpu.roll(x, hd // 2, 1) * sine) * scale)
        return parts

    queries = rotated(projected(0), 1.0)
    keys = rotated(projected(1), hd ** (-0.5))
    for h in range(heads):
        padded[h, 0:rows_k, :] = queries[h]
        key_out_ref[:, h * hd : (h + 1) * hd] = keys[h]
    for h in range(heads):
        turned = padded[h].T
        for s in range(rows_k):
            carried[h, s : s + 1, :] = jnp.sum(turned[:, s : s + 1] * state[s, h], axis=0, keepdims=True)
    values = projected(2)
    value_out_ref[...] = values
    gates = silu(projected(3))
    for h in range(heads):
        head = slice(h * hd, (h + 1) * hd)
        exponent = jnp.full((1, hd), me_t * heads + h, jnp.int32).astype(F32)
        decay = 1.0 - jnp.exp2(-5.0 - exponent)
        within = jnp.sum(queries[h] * keys[h], axis=1, keepdims=True)
        mixture = decay * carried[h, 0:rows_k, :] + within * values[:, head]
        centered = mixture - jnp.mean(mixture, axis=1, keepdims=True)
        variance = jnp.mean(centered * centered, axis=1, keepdims=True)
        normed = centered * lax.rsqrt(variance + EPS_GROUP) * head_gain_ref[:, head]
        ret_slots[me_k, :, head] = (gates[:, head] * normed).astype(BF16)
    ret_arrive = exchange(
        "kv", me_k, kv, lambda dest: ret_slots.at[me_k], ret_slots, ret_send_sem, ret_recv_sem
    )
    loads[8].wait()
    ret_arrive()
    for k in range(kv):
        mixed[k * rows_k : (k + 1) * rows_k, :] = ret_slots[k].astype(F32)
    acc[...] = jnp.dot(mixed[...].astype(BF16), wo[...], preferred_element_type=F32)
    arrive = advance(1, 1.0, False)
    finish2 = feed_forward(1, 2, arrive, gain2_ref, gate2, up2, down2, loads[9:12])
    advance(2, 0.5, True)
    finish1()
    finish2()
    for copy in pending:
        copy.wait_send()


def solution(mesh):
    kv, tp = mesh.shape["kv"], mesh.shape["tp"]

    def per_device(
        stream_in, positions, ret_state, first_gain, first_gate, first_up, first_down, mix_gain,
        w_query, w_key, w_value, w_outgate, w_out, head_gain, second_gain, second_gate, second_up,
        second_down,
    ):
        rows_t, width = stream_in.shape
        rows = rows_t * tp
        seqs, heads, hd, _ = ret_state.shape
        qw = heads * hd
        units = first_gate.shape[1]
        share = -(-(-(-units // PIECE)) // kv)
        half_dim = hd // 2
        freq = 10000.0 ** (-jnp.arange(half_dim, dtype=F32) / half_dim)
        angles = positions.astype(F32)[:, None] * freq[None, :]
        cosine, sine = jnp.cos(angles), jnp.sin(angles)
        cosine = jnp.concatenate([cosine, cosine], axis=1)
        sine = jnp.concatenate([-sine, sine], axis=1)
        weights = (
            first_gate, first_up, first_down, w_query, w_key, w_value, w_outgate, w_out,
            second_gate, second_up, second_down,
        )
        vmem = pl.BlockSpec(memory_space=pltpu.VMEM)
        anywhere = pl.BlockSpec(memory_space=pl.ANY)
        dma = pltpu.SemaphoreType.DMA
        pad_rows = -(-seqs // 16) * 16
        out, keys, values = pl.pallas_call(
            functools.partial(layer_kernel, kv, tp, share),
            out_shape=(
                jax.ShapeDtypeStruct((rows_t, width), BF16),
                jax.ShapeDtypeStruct((seqs, qw), F32),
                jax.ShapeDtypeStruct((seqs, qw), F32),
            ),
            in_specs=[vmem] * 7 + [anywhere] * 12,
            out_specs=(vmem, vmem, vmem),
            scratch_shapes=[pltpu.VMEM(w.shape, BF16) for w in weights]
            + [
                pltpu.VMEM(ret_state.shape, F32),
                pltpu.VMEM((3, tp, rows_t, width), BF16),
                pltpu.VMEM((3, tp, rows_t, width), BF16),
                pltpu.VMEM((3, tp, rows_t, width), BF16),
                pltpu.VMEM((rows, width), F32),
                pltpu.VMEM((rows, width), BF16),
                pltpu.VMEM((rows, width), F32),
                pltpu.VMEM((2, kv, rows, 128), F32),
                pltpu.VMEM((rows, 128), F32),
                pltpu.VMEM((2, kv, share, 2, rows, PIECE), BF16),
                pltpu.VMEM((2, kv, share, 2, rows, PIECE), BF16),
                pltpu.VMEM((2, kv * share, rows, PIECE), BF16),
                pltpu.VMEM((rows, qw), F32),
                pltpu.VMEM((4, kv, seqs, qw), BF16),
                pltpu.VMEM((4, kv, seqs, qw), BF16),
                pltpu.VMEM((rows, 128), F32),
                pltpu.VMEM((kv, seqs, 128), F32),
                pltpu.VMEM((kv, seqs, 128), F32),
                pltpu.VMEM((heads, pad_rows, hd), F32),
                pltpu.VMEM((heads, pad_rows, hd), F32),
                pltpu.VMEM((kv, seqs, qw), BF16),
                pltpu.VMEM((rows, qw), F32),
                dma((12,)), dma((6, tp)), dma((6, tp)), dma((2, kv)), dma((2, kv)),
                dma((2, kv, share)), dma((2, kv, share)), dma((2, kv, share)), dma((2, kv, share)),
                dma((4, kv)), dma((4, kv)), dma((kv,)), dma((kv,)), dma((kv,)), dma((kv,)),
            ],
            compiler_params=pltpu.CompilerParams(
                collective_id=0, has_side_effects=True, vmem_limit_bytes=63 * 1024 * 1024
            ),
        )(
            stream_in, cosine, sine, first_gain[None, :], mix_gain[None, :], second_gain[None, :],
            head_gain[None, :], *weights[0:8], *weights[8:11], ret_state,
        )
        head_ids = (lax.axis_index("tp") * heads + jnp.arange(heads)).astype(F32)
        decays = 1.0 - 2.0 ** (-5.0 - head_ids)
        keys = keys.reshape(seqs, heads, hd)
        values = values.reshape(seqs, heads, hd)
        new_state = (
            decays[None, :, None, None] * ret_state + keys[..., :, None] * values[..., None, :]
        )
        return out, new_state

    in_specs = (
        P(("grp", "tp"), "kv"), P(("grp", "kv")), P(("grp", "kv"), "tp", None, None), P("kv"),
        P("kv", "tp"), P("kv", "tp"), P("tp", "kv"), P("kv"), P("kv", "tp"), P("kv", "tp"),
        P("kv", "tp"), P("kv", "tp"), P("tp", "kv"), P("tp"), P("kv"), P("kv", "tp"),
        P("kv", "tp"), P("tp", "kv"),
    )
    out_specs = (P(("grp", "tp"), "kv"), P(("grp", "kv"), "tp", None, None))
    return jax.shard_map(
        per_device, mesh=mesh, in_specs=in_specs, out_specs=out_specs, check_vma=False
    )
```

time: 237 us -> 129 us (0.54)
  blocking collectives: 103 us -> 0 us
  Pallas kernels: 0 us -> 86.4 us
  waiting for transfers between devices: 57.8 us -> 0 us
  matrix products: 34.3 us -> 0 us
  local copies, waits for them, and re-layouts: 2.53 us -> 35.5 us
  between operations: 16.5 us -> 0.67 us
  starting transfers between devices: 15.1 us -> 0 us
    pallas_call x0 -> x1, Pallas kernels: none -> 86.4 us  [per_device(): pl.pallas_call(functools.partial(layer_kernel, kv, tp, share), out_shape=...]
    psum x2 -> x0, waiting for transfers between devices: 56.1 us -> none  [feed_forward(): lax.psum(up_part.astype(jnp.bfloat16), 'kv').astype(jnp.float32)]
    unnamed x5 -> x0, blocking collectives: 46.3 us -> none
    dot_general x12 -> x0, matrix products: 34.3 us -> none  [the longest x2 10.4 us: feed_forward(): up_part = jnp.dot(scaled, w_up, preferred_element_type=jnp.float32)]
    all_gather x4 -> x0, blocking collectives: 33.3 us -> none  [the longest x3 20.1 us: widen_rows(): return lax.all_gather(stream_rows, 'tp', axis=0, tiled=True)]
    unnamed x43 -> x7, local copies, waits for them, and re-layouts: 2.47 us -> 34 us
    psum x2 -> x0, blocking collectives: 23.3 us -> none  [feed_forward(): lax.psum(squares.astype(jnp.bfloat16), 'kv').astype(jnp.float32)]
    unnamed x7 -> x0, starting transfers between devices: 15 us -> none
  transfers between devices with their start and end apart: 9 -> 0, of which waited for: 4 -> 0; matrix products, arithmetic and copies ran while one was open for 2% -> 0% of each run, Pallas kernels for 0% -> 0%
where the time goes in v1:
time: 129 us; the launch traced here: 128 us
  Pallas kernels  86.4 us (67%)
  local copies, waits for them, and re-layouts  35.5 us (28%)
  other arithmetic  5.04 us (4%)
    pallas_call x1, Pallas kernels, per_device(): pl.pallas_call(functools.partial(layer_kernel, kv, tp, share), out_shape=...  86.4 us
    unnamed x7, local copies, waits for them, and re-layouts  34 us
    add x1, other arithmetic, per_device(): decays[None, :, None, None] * ret_state  3.57 us

profile of v1, /device:TPU:0, one launch (start us, length us, event | category | flops | bytes accessed | tf_op | source)
XLA Modules:
  0.0 127.7 jit_solution(5811594475244690517)
XLA Ops:
  0.6 0.7 convert_element_type.10
  1.3 0.1 fusion
  1.4 0.7 pad_maximum_fusion
  2.1 8.3 %copy.20.gate1_hbm = bf16[1024,2752]{1,0:T(8,128)(2,1)} copy(bf16[1024,2752]{0,1:T(8,128)(2,1)} %param.22) | data formatting | bytes 11272192 | tf_op args[4]
  10.5 8.4 %copy.21.up1_hbm = bf16[1024,2752]{1,0:T(8,128)(2,1)} copy(bf16[1024,2752]{0,1:T(8,128)(2,1)} %param.23) | data formatting | bytes 11272192 | tf_op args[5]
  18.9 8.3 %copy.22.gate2_hbm = bf16[1024,2752]{1,0:T(8,128)(2,1)} copy(bf16[1024,2752]{0,1:T(8,128)(2,1)} %param.33) | data formatting | bytes 11272192 | tf_op args[15]
  27.2 8.3 %copy.23.up2_hbm = bf16[1024,2752]{1,0:T(8,128)(2,1)} copy(bf16[1024,2752]{0,1:T(8,128)(2,1)} %param.34) | data formatting | bytes 11272192 | tf_op args[16]
  35.5 86.4 %shard_map.185 = (bf16[12,1024]{1,0:T(8,128)(2,1)}, f32[12,512]{1,0:T(8,128)}, f32[12,512]{1,0:T(8,128)}) custom-call(bf16[12,1024]{1,0:T(8,128)(2,1)} %stream_ref.1, f32[12,128]{1,0:T(8,128)} %get-tuple-element.11.cos_ref, f32[12,128]{1,0:T(8,128)} %get-tuple-element.12.sin_ref, f32[1,1024]{1,0:T(1,128)} %bitcast.4, f32[1,1024]{1,0:T(1,128)} %bitcast.5, ...), custom_call_target="tpu_custom_call" | custom-call | tf_op jit(solution)/shard_map/pallas_call | solution.py:385
  121.9 0.0 copy-start
  121.9 0.8 mul.47
  122.7 0.8 mul.49
  123.5 3.6 %multiply_add_fusion = f32[12,4,128,128]{3,2,1,0:T(8,128)} fusion(f32[12,4,128,128]{3,2,1,0:T(8,128)} %state_hbm.1, f32[12,4,128]{2,1,0:T(4,128)S(1)} %mul.49, f32[12,4,128]{2,1,0:T(4,128)S(1)} %mul.47, f32[4]{0:T(128)S(1)} %power_subtract_fusion), kind=kLoop, calls=%fused_computation | loop fusion | flops 2359296 | bytes 6340624 | tf_op jit(solution)/shard_map/add | solution.py:434
  127.1 0.0 copy-done
  127.1 0.6 copy.25
  (2 shorter events, 0.0 us)
Async XLA Ops:
  121.9 5.1 %copy-start = (bf16[12,1024]{1,0:T(8,128)(2,1)S(1)}, bf16[12,1024]{1,0:T(8,128)(2,1)}, u32[]{:S(2)}) copy-start(bf16[12,1024]{1,0:T(8,128)(2,1)} %get-tuple-element.15) | copy-start | bytes 73732

commit v2 on v1

--- a/solution.py
+++ b/solution.py
@@ -38,7 +38,7 @@
     me_t = lax.axis_index("tp")
     rows, width = wide.shape
     model = width * kv
-    units = gate1.shape[1]
+    units = gate1.shape[0]
     pieces = -(-units // PIECE)
     ragged = units - (pieces - 1) * PIECE
     rows_t = rows // tp
@@ -146,15 +146,15 @@
             )
 
         def on_piece(i, _):
-            dest = order_of(i // share)
-            p = lax.rem(i, share)
+            dest = order_of(lax.rem(i, kv))
+            p = i // kv
             g = dest * share + p
 
             def multiply(columns, n):
                 left = lhs[...]
                 for which, w in enumerate((w_gate, w_up)):
-                    ff_send[block, dest, p, which, :, 0:n] = jnp.dot(
-                        left, w[:, columns], preferred_element_type=F32
+                    ff_send[block, dest, p, which, :, 0:n] = lax.dot_general(
+                        left, w[columns, :], (((1,), (1,)), ((), ())), preferred_element_type=F32
                     ).astype(BF16)
 
             @pl.when(g < pieces - 1)
@@ -218,8 +218,8 @@
         waits[2].wait()
 
         def on_hidden(i, _):
-            source = order_of(kv - 1 - i // share)
-            p = lax.rem(i, share)
+            source = order_of(kv - 1 - lax.rem(i, kv))
+            p = i // kv
             g = source * share + p
 
             @pl.when((g < pieces) & (source != me_k))
@@ -375,8 +375,8 @@
         cosine = jnp.concatenate([cosine, cosine], axis=1)
         sine = jnp.concatenate([-sine, sine], axis=1)
         weights = (
-            first_gate, first_up, first_down, w_query, w_key, w_value, w_outgate, w_out,
-            second_gate, second_up, second_down,
+            first_gate.T, first_up.T, first_down, w_query, w_key, w_value, w_outgate, w_out,
+            second_gate.T, second_up.T, second_down,
         )
         vmem = pl.BlockSpec(memory_space=pltpu.VMEM)
         anywhere = pl.BlockSpec(memory_space=pl.ANY)

time: 129 us -> 94.6 us (0.73)
  local copies, waits for them, and re-layouts: 35.5 us -> 2.16 us
    unnamed x7 -> x3, local copies, waits for them, and re-layouts: 34 us -> 0.62 us
where the time goes in v2:
time: 94.6 us; the launch traced here: 94.3 us
  Pallas kernels  86.4 us (91%)
  other arithmetic  5.04 us (5%)
  local copies, waits for them, and re-layouts  2.16 us (2%)
    pallas_call x1, Pallas kernels, per_device(): pl.pallas_call(functools.partial(layer_kernel, kv, tp, share), out_shape=...  86.4 us
    add x1, other arithmetic, per_device(): decays[None, :, None, None] * ret_state  3.57 us

profile of v2, /device:TPU:0, one launch (start us, length us, event | category | flops | bytes accessed | tf_op | source)
XLA Modules:
  0.0 94.3 jit_solution(12805834732859155880)
XLA Ops:
  0.6 0.7 convert_element_type.10
  1.3 0.1 fusion
  1.4 0.7 pad_maximum_fusion
  2.1 86.4 %shard_map.185 = (bf16[12,1024]{1,0:T(8,128)(2,1)}, f32[12,512]{1,0:T(8,128)}, f32[12,512]{1,0:T(8,128)}) custom-call(bf16[12,1024]{1,0:T(8,128)(2,1)} %stream_ref.1, f32[12,128]{1,0:T(8,128)} %get-tuple-element.11.cos_ref, f32[12,128]{1,0:T(8,128)} %get-tuple-element.12.sin_ref, f32[1,1024]{1,0:T(1,128)} %bitcast.12, f32[1,1024]{1,0:T(1,128)} %bitcast.13, ...), custom_call_target="tpu_custom_call" | custom-call | tf_op jit(solution)/shard_map/pallas_call | solution.py:385
  88.5 0.8 mul.47
  89.3 0.8 mul.49
  90.1 0.0 copy-start
  90.1 3.6 %multiply_add_fusion = f32[12,4,128,128]{3,2,1,0:T(8,128)} fusion(f32[12,4,128,128]{3,2,1,0:T(8,128)} %state_hbm.1, f32[12,4,128]{2,1,0:T(4,128)S(1)} %mul.49, f32[12,4,128]{2,1,0:T(4,128)S(1)} %mul.47, f32[4]{0:T(128)S(1)} %power_subtract_fusion), kind=kLoop, calls=%fused_computation | loop fusion | flops 2359296 | bytes 6340624 | tf_op jit(solution)/shard_map/add | solution.py:434
  93.7 0.0 copy-done
  93.7 0.6 copy.21
  (2 shorter events, 0.0 us)
Async XLA Ops:
  90.1 3.6 %copy-start = (bf16[12,1024]{1,0:T(8,128)(2,1)S(1)}, bf16[12,1024]{1,0:T(8,128)(2,1)}, u32[]{:S(2)}) copy-start(bf16[12,1024]{1,0:T(8,128)(2,1)} %get-tuple-element.15) | copy-start | bytes 73732

commit v3 on v2

--- a/solution.py
+++ b/solution.py
@@ -22,14 +22,14 @@
 
 def layer_kernel(
     kv, tp, share,
-    stream_ref, cos_ref, sin_ref, gain1_ref, gain_mix_ref, gain2_ref, head_gain_ref,
+    stream_ref, freq_ref, sign_ref, pos_ref, gain1_ref, gain_mix_ref, gain2_ref, head_gain_ref,
     gate1_hbm, up1_hbm, down1_hbm, wq_hbm, wk_hbm, wv_hbm, wg_hbm, wo_hbm,
     gate2_hbm, up2_hbm, down2_hbm, state_hbm,
     out_ref, key_out_ref, value_out_ref,
     gate1, up1, down1, wq, wk, wv, wg, wo, gate2, up2, down2, state,
     stream_slots, part_send, part_recv, wide, lhs, acc, sq_slots, inverse,
     ff_send, ff_recv, hidden, proj, proj_send, proj_recv, row_sq, row_sq_send, row_sq_recv,
-    padded, carried, ret_slots, mixed,
+    padded, carried, ret_slots, mixed, angles, turns,
     load_sem, tp_send_sem, tp_recv_sem, sq_send_sem, sq_recv_sem,
     ff_send_sem, ff_recv_sem, hid_send_sem, hid_recv_sem,
     proj_send_sem, proj_recv_sem, row_send_sem, row_recv_sem, ret_send_sem, ret_recv_sem,
@@ -270,6 +270,11 @@
 
     stream_slots[0, me_t] = stream_ref[...]
     arrive = gather_stream(0)
+    for s in range(rows_k):
+        angles[s : s + 1, :] = freq_ref[...] * jnp.full((1, hd), pos_ref[s], jnp.int32).astype(F32)
+    turn = angles[0:rows_k, :]
+    turns[0] = jnp.cos(turn)
+    turns[1] = jnp.sin(turn) * sign_ref[...]
     finish1 = feed_forward(0, 0, arrive, gain1_ref, gate1, up1, down1, loads[0:3])
     arrive = advance(0, 0.5, False)
 
@@ -306,7 +311,8 @@
             value = value + proj_recv[n, lax.rem(me_k + j, kv)].astype(F32)
         return value * factor
 
-    cosine, sine = cos_ref[...], sin_ref[...]
+
+    cosine, sine = turns[0], turns[1]
 
     def rotated(value, scale):
         parts = []
@@ -319,7 +325,8 @@
     keys = rotated(projected(1), hd ** (-0.5))
     for h in range(heads):
         padded[h, 0:rows_k, :] = queries[h]
-        key_out_ref[:, h * hd : (h + 1) * hd] = keys[h]
+        padded[heads + h, 0:rows_k, :] = keys[h]
+        key_out_ref[h] = padded[heads + h].T
     for h in range(heads):
         turned = padded[h].T
         for s in range(rows_k):
@@ -329,8 +336,7 @@
     gates = silu(projected(3))
     for h in range(heads):
         head = slice(h * hd, (h + 1) * hd)
-        exponent = jnp.full((1, hd), me_t * heads + h, jnp.int32).astype(F32)
-        decay = 1.0 - jnp.exp2(-5.0 - exponent)
+        decay = decay_of(me_t * heads + h, hd)
         within = jnp.sum(queries[h] * keys[h], axis=1, keepdims=True)
         mixture = decay * carried[h, 0:rows_k, :] + within * values[:, head]
         centered = mixture - jnp.mean(mixture, axis=1, keepdims=True)
@@ -354,6 +360,16 @@
         copy.wait_send()
 
 
+def decay_of(head, width):
+    return 1.0 - jnp.exp2(-5.0 - jnp.full((1, width), head, jnp.int32).astype(F32))
+
+
+def state_kernel(heads, key_ref, value_ref, state_ref, new_ref):
+    decay = decay_of(lax.axis_index("tp") * heads + pl.program_id(0), state_ref.shape[3])
+    for s in range(state_ref.shape[0]):
+        new_ref[s, 0] = decay * state_ref[s, 0] + key_ref[0, :, s : s + 1] * value_ref[s : s + 1, :]
+
+
 def solution(mesh):
     kv, tp = mesh.shape["kv"], mesh.shape["tp"]
 
@@ -369,11 +385,9 @@
         units = first_gate.shape[1]
         share = -(-(-(-units // PIECE)) // kv)
         half_dim = hd // 2
-        freq = 10000.0 ** (-jnp.arange(half_dim, dtype=F32) / half_dim)
-        angles = positions.astype(F32)[:, None] * freq[None, :]
-        cosine, sine = jnp.cos(angles), jnp.sin(angles)
-        cosine = jnp.concatenate([cosine, cosine], axis=1)
-        sine = jnp.concatenate([-sine, sine], axis=1)
+        freq = (10000.0 ** (-np.arange(half_dim, dtype=np.float64) / half_dim)).astype(np.float32)
+        freq = np.concatenate([freq, freq])[None, :]
+        sign = np.concatenate([-np.ones(half_dim), np.ones(half_dim)])[None, :].astype(np.float32)
         weights = (
             first_gate.T, first_up.T, first_down, w_query, w_key, w_value, w_outgate, w_out,
             second_gate.T, second_up.T, second_down,
@@ -386,10 +400,10 @@
             functools.partial(layer_kernel, kv, tp, share),
             out_shape=(
                 jax.ShapeDtypeStruct((rows_t, width), BF16),
-                jax.ShapeDtypeStruct((seqs, qw), F32),
+                jax.ShapeDtypeStruct((heads, hd, pad_rows), F32),
                 jax.ShapeDtypeStruct((seqs, qw), F32),
             ),
-            in_specs=[vmem] * 7 + [anywhere] * 12,
+            in_specs=[vmem] * 3 + [pl.BlockSpec(memory_space=pltpu.SMEM)] + [vmem] * 4 + [anywhere] * 12,
             out_specs=(vmem, vmem, vmem),
             scratch_shapes=[pltpu.VMEM(w.shape, BF16) for w in weights]
             + [
@@ -411,10 +425,12 @@
                 pltpu.VMEM((rows, 128), F32),
                 pltpu.VMEM((kv, seqs, 128), F32),
                 pltpu.VMEM((kv, seqs, 128), F32),
-                pltpu.VMEM((heads, pad_rows, hd), F32),
+                pltpu.VMEM((2 * heads, pad_rows, hd), F32),
                 pltpu.VMEM((heads, pad_rows, hd), F32),
                 pltpu.VMEM((kv, seqs, qw), BF16),
                 pltpu.VMEM((rows, qw), F32),
+                pltpu.VMEM((pad_rows, hd), F32),
+                pltpu.VMEM((2, seqs, hd), F32),
                 dma((12,)), dma((6, tp)), dma((6, tp)), dma((2, kv)), dma((2, kv)),
                 dma((2, kv, share)), dma((2, kv, share)), dma((2, kv, share)), dma((2, kv, share)),
                 dma((4, kv)), dma((4, kv)), dma((kv,)), dma((kv,)), dma((kv,)), dma((kv,)),
@@ -423,16 +439,22 @@
                 collective_id=0, has_side_effects=True, vmem_limit_bytes=63 * 1024 * 1024
             ),
         )(
-            stream_in, cosine, sine, first_gain[None, :], mix_gain[None, :], second_gain[None, :],
+            stream_in, freq, sign, positions, first_gain[None, :], mix_gain[None, :], second_gain[None, :],
             head_gain[None, :], *weights[0:8], *weights[8:11], ret_state,
         )
-        head_ids = (lax.axis_index("tp") * heads + jnp.arange(heads)).astype(F32)
-        decays = 1.0 - 2.0 ** (-5.0 - head_ids)
-        keys = keys.reshape(seqs, heads, hd)
-        values = values.reshape(seqs, heads, hd)
-        new_state = (
-            decays[None, :, None, None] * ret_state + keys[..., :, None] * values[..., None, :]
-        )
+        one = lambda h: (0, h, 0, 0)
+        new_state = pl.pallas_call(
+            functools.partial(state_kernel, heads),
+            grid=(heads,),
+            out_shape=jax.ShapeDtypeStruct(ret_state.shape, F32),
+            in_specs=[
+                pl.BlockSpec((1, hd, pad_rows), lambda h: (h, 0, 0)),
+                pl.BlockSpec((seqs, hd), lambda h: (0, h)),
+                pl.BlockSpec((seqs, 1, hd, hd), one),
+            ],
+            out_specs=pl.BlockSpec((seqs, 1, hd, hd), one),
+            compiler_params=pltpu.CompilerParams(dimension_semantics=("arbitrary",)),
+        )(keys, values, ret_state)
         return out, new_state
 
     in_specs = (

time: 94.6 us -> 92.9 us (0.982)
  other arithmetic: 5.04 us -> 0 us
  Pallas kernels: 86.4 us -> 91.4 us
  local copies, waits for them, and re-layouts: 2.16 us -> 0.62 us
    pallas_call x0 -> x1, Pallas kernels: none -> 4.78 us  [per_device(): pl.pallas_call(functools.partial(state_kernel, heads), grid=(heads,), out...]
    add x1 -> x0, other arithmetic: 3.57 us -> none  [per_device(): decays[None, :, None, None] * ret_state]
    mul x2 -> x0, local copies, waits for them, and re-layouts: 1.54 us -> none  [per_device(): keys[..., :, None] * values[..., None, :]]
where the time goes in v3:
time: 92.9 us; the launch traced here: 92.6 us
  Pallas kernels  91.4 us (98%)
    pallas_call x1, Pallas kernels, per_device(): pl.pallas_call(functools.partial(layer_kernel, kv, tp, share), out_shape=...  86.6 us
    pallas_call x1, Pallas kernels, per_device(): pl.pallas_call(functools.partial(state_kernel, heads), grid=(heads,), out...  4.78 us

profile of v3, /device:TPU:0, one launch (start us, length us, event | category | flops | bytes accessed | tf_op | source)
XLA Modules:
  0.0 92.6 jit_solution(4896464466475450061)
XLA Ops:
  0.6 86.6 %shard_map.203 = (bf16[12,1024]{1,0:T(8,128)(2,1)}, f32[4,128,16]{2,1,0:T(8,128)}, f32[12,512]{1,0:T(8,128)}) custom-call(bf16[12,1024]{1,0:T(8,128)(2,1)} %stream_ref.1, f32[1,128]{1,0:T(1,128)} %constant.4.clone.freq_ref, f32[1,128]{1,0:T(1,128)} %constant.5.clone.sign_ref, s32[12]{0:T(128)} %pos_ref.1, f32[1,1024]{1,0:T(1,128)} %bitcast.12, ...), custom_call_target="tpu_custom_call" | custom-call | tf_op jit(solution)/shard_map/pallas_call | solution.py:399
  87.2 0.0 copy-start
  87.2 4.8 %shard_map.204 = f32[12,4,128,128]{3,2,1,0:T(8,128)} custom-call(f32[4,128,16]{2,1,0:T(8,128)} %get-tuple-element.6.key_ref, f32[12,512]{1,0:T(8,128)} %get-tuple-element.7.value_ref, f32[12,4,128,128]{3,2,1,0:T(8,128)} %state_ref.1), custom_call_target="tpu_custom_call" | custom-call | tf_op jit(solution)/shard_map/pallas_call | solution.py:446
  92.0 0.0 copy-done
  92.0 0.6 copy.23
Async XLA Ops:
  87.2 4.8 %copy-start = (bf16[12,1024]{1,0:T(8,128)(2,1)S(1)}, bf16[12,1024]{1,0:T(8,128)(2,1)}, u32[]{:S(2)}) copy-start(bf16[12,1024]{1,0:T(8,128)(2,1)} %get-tuple-element.10) | copy-start | bytes 73732
